TPU v7x, 32 devices: a whole 2x2x4 slice. The times are simulated.
32 devices in a mesh: sp: 8 (over z, core), tp: 4 (over y, x).
Axes of the slice: x: 2, y: 2, z: 4, core: 2. Of those that a mesh axis runs over, the one named last changes fastest.
Arguments:
- resid: bfloat16 [1536, 2048], P('sp', 'tp'), may hold values from -12 to 12
- conv_value: bfloat16 [1536, 2048], P('sp', 'tp'), may hold values from -80 to 80
- conv_gate: bfloat16 [1536, 2048], P('sp', 'tp'), may hold values from -6 to 6
- depth_kernel: float32 [31, 2048], P(None, 'tp'), may hold values from -1 to 1
- chan_gain: float32 [2048], P('tp'), may hold values from 0.1 to 1.9
- point_weight: bfloat16 [2048, 2048], P('tp'), may hold values from -0.125 to 0.125
- mix_gain: float32 [2048], replicated, may hold values from 0.1 to 1.9
- out_weight: bfloat16 [2048, 2048], P(None, 'tp'), may hold values from -0.125 to 0.125
- norm_gain: float32 [2048], P('tp'), may hold values from 0.1 to 1.9
- route_ids: int32 [1536, 4], P('sp'), may hold values from 0 to 31, all different within a row; in each aligned block of 192 rows (0 to 191, 192 to 383, ...) at most 32 rows name the same one
- route_weights: float32 [1536, 4], P('sp'), may hold values from 0.05 to 0.5
- gate_experts: bfloat16 [32, 2048, 4096], P('sp', None, 'tp'), may hold values from -0.3125 to 0.3125
- up_experts: bfloat16 [32, 2048, 4096], P('sp', None, 'tp'), may hold values from -0.3125 to 0.3125
- down_experts: bfloat16 [32, 4096, 2048], P('sp', 'tp'), may hold values from -0.09375 to 0.09375
Outputs:
- result: bfloat16 [1536, 2048], P('sp', 'tp')
Inputs may be any that keep to these rules, and one draw needn't show every extreme that they name: `route_ids`: each row names 4 different experts; among the 192 rows of one index of sp no expert is named by more than 32 rows, and in some such block an expert is named by exactly 32.
All inputs are finite; a program needn't handle non-finite values.
Results may differ from a plain program's by a relative error of at most 0.024.
Values may be sent and summed in bfloat16 or wider, within the bound.
No kernel may reach another device: no remote copies, remote signals or barrier semaphores. Data moves between devices by JAX's collectives and lax.ppermute only.
A program may use at most 128 MiB of HBM per device.

v0:
```python
import jax
import jax.numpy as jnp
from jax import lax
from jax.sharding import PartitionSpec as P

E = 32
TOPK = 4
CAP = 32
epsilon = 1e-05
clamp_limit = 7.0
swish_slope = 1.702


def from_behind(block, axis, distance):
    devices = range(lax.axis_size(axis))
    route = [(i - distance, i) for i in devices if i - distance in devices]
    return lax.ppermute(block, axis, route)


def shards(
    resid,
    conv_value,
    conv_gate,
    depth_kernel,
    chan_gain,
    point_weight,
    mix_gain,
    out_weight,
    norm_gain,
    route_ids,
    route_weights,
    gate_experts,
    up_experts,
    down_experts,
):
    tok_rows, chan_local = conv_value.shape
    feat_local = resid.shape[1]
    lookback = depth_kernel.shape[0] - 1
    gated = (conv_value.astype(jnp.float32) * jax.nn.sigmoid(conv_gate.astype(jnp.float32))).astype(
        jnp.bfloat16
    )
    earlier = from_behind(gated[tok_rows - lookback :], "sp", 1)
    padded = jnp.concatenate([earlier, gated], axis=0)
    conv = jnp.zeros((tok_rows, chan_local), jnp.float32)
    for tap in range(lookback + 1):
        conv = conv + padded[tap : tap + tok_rows].astype(jnp.float32) * depth_kernel[tap]
    chan_total = chan_local * lax.axis_size("tp")
    row_sums, row_squares = lax.psum((jnp.sum(conv, axis=1), jnp.sum(conv * conv, axis=1)), "tp")
    row_mean = row_sums / chan_total
    row_var = row_squares / chan_total - row_mean * row_mean
    act = jax.nn.silu(
        (conv - row_mean[:, None]) * lax.rsqrt(row_var[:, None] + epsilon) * chan_gain
    ).astype(jnp.bfloat16)
    point = lax.psum_scatter(
        jnp.dot(act, point_weight, preferred_element_type=jnp.float32).astype(jnp.bfloat16),
        "tp",
        scatter_dimension=0,
        tiled=True,
    ).astype(jnp.float32)
    mixed = (
        point * lax.rsqrt(jnp.mean(point * point, axis=1, keepdims=True) + epsilon) * mix_gain
    ).astype(jnp.bfloat16)
    branch = jnp.dot(
        lax.all_gather(mixed, "tp", axis=0, tiled=True),
        out_weight,
        preferred_element_type=jnp.float32,
    )
    middle = (resid.astype(jnp.float32) + branch).astype(jnp.bfloat16)
    middle32 = middle.astype(jnp.float32)
    feat_total = feat_local * lax.axis_size("tp")
    squares = lax.psum(jnp.sum(middle32 * middle32, axis=1), "tp")
    normed = (middle32 * lax.rsqrt(squares[:, None] / feat_total + epsilon) * norm_gain).astype(
        jnp.bfloat16
    )
    flat_ids = route_ids.reshape(-1)
    expert_table = (flat_ids[:, None] == jnp.arange(E, dtype=jnp.int32)[None, :]).astype(jnp.int32)
    earlier_count = jnp.cumsum(expert_table, axis=0) - expert_table
    position = jnp.sum(earlier_count * expert_table, axis=1)
    slot_of = flat_ids * CAP + position
    slot_grid = slot_of.reshape(tok_rows, TOPK)
    picker = jnp.any(
        slot_grid[None, :, :] == jnp.arange(E * CAP, dtype=jnp.int32)[:, None, None], axis=2
    ).astype(jnp.bfloat16)
    outgoing = (
        jnp.dot(picker, normed, preferred_element_type=jnp.float32)
        .astype(jnp.bfloat16)
        .reshape(E, CAP, feat_local)
    )
    received = lax.all_gather(
        lax.all_to_all(outgoing, "sp", split_axis=0, concat_axis=0, tiled=True),
        "tp",
        axis=2,
        tiled=True,
    )
    local_experts = gate_experts.shape[0]
    sources = received.shape[0] // local_experts
    count = received.shape[1]
    rows = received.reshape(sources, local_experts, count, received.shape[2])
    gate_pre = jnp.minimum(
        jnp.einsum("sjcd,jdf->sjcf", rows, gate_experts, preferred_element_type=jnp.float32),
        clamp_limit,
    )
    up_pre = jnp.clip(
        jnp.einsum("sjcd,jdf->sjcf", rows, up_experts, preferred_element_type=jnp.float32),
        -clamp_limit,
        clamp_limit,
    )
    hidden = (gate_pre * jax.nn.sigmoid(swish_slope * gate_pre) * (up_pre + 1.0)).astype(
        jnp.bfloat16
    )
    partial_value = jnp.einsum(
        "sjcf,jfd->sjcd", hidden, down_experts, preferred_element_type=jnp.float32
    )
    summed = lax.psum_scatter(
        partial_value.astype(jnp.bfloat16), "tp", scatter_dimension=3, tiled=True
    )
    returned = lax.all_to_all(
        summed.reshape(sources * local_experts, count, summed.shape[3]),
        "sp",
        split_axis=0,
        concat_axis=0,
        tiled=True,
    )
    flat_back = returned.reshape(E * CAP, feat_local)
    picked = flat_back[slot_of].astype(jnp.float32).reshape(tok_rows, TOPK, feat_local)
    routed_sum = jnp.sum(picked * route_weights[:, :, None], axis=1)
    return (middle32 + routed_sum).astype(jnp.bfloat16)


def solution(mesh):
    in_specs = (
        P("sp", "tp"),
        P("sp", "tp"),
        P("sp", "tp"),
        P(None, "tp"),
        P("tp"),
        P("tp", None),
        P(),
        P(None, "tp"),
        P("tp"),
        P("sp", None),
        P("sp", None),
        P("sp", None, "tp"),
        P("sp", None, "tp"),
        P("sp", "tp", None),
    )
    out_specs = P("sp", "tp")
    return jax.shard_map(shards, mesh=mesh, in_specs=in_specs, out_specs=out_specs, check_vma=False)
```

profile of v0, /device:TPU:0, one launch (start us, length us, event | category | flops | bytes accessed | tf_op | source)
XLA Modules:
  0.0 297.5 jit_solution(6796532725709463423)
XLA Ops:
  6.5 1.3 multiply_convert_fusion.2
  7.9 2.4 collective-permute-start
  10.3 1.3 fusion.68
  11.5 1.1 fusion.69
  12.6 2.2 fusion.67
  14.9 10.9 %all-reduce = (f32[192]{0:T(256)S(1)}, f32[192]{0:T(256)S(1)}) all-reduce(f32[192]{0:T(256)S(1)} %get-tuple-element.6, f32[192]{0:T(256)S(1)} %get-tuple-element.5), channel_id=1, replica_groups=mesh['sp'=8,'tp'=4] {'tp'}, use_global_device_ids=true, to_apply=%region_3.0 | all-reduce | flops 384 | bytes 3072 | tf_op jit(solution)/shard_map/psum | solution.py:48
  25.8 2.2 convolution_convert_fusion
  28.5 1.7 reduce-window.6
  31.4 23.3 %reduce-scatter.3.cloned.1.call-done = bf16[48,2048]{1,0:T(8,128)(2,1)} async-done(((bf16[192,2048]{1,0:T(8,128)(2,1)}), bf16[48,2048]{1,0:T(8,128)(2,1)}) %reduce-scatter.3.cloned.1.call-update) | async-done | bytes 196624 | tf_op jit(solution)/shard_map/reduce_scatter | solution.py:54
  56.8 11.2 %all_gather.6 = bf16[192,2048]{1,0:T(8,128)(2,1)S(1)} all-gather(bf16[48,2048]{1,0:T(8,128)(2,1)S(1)} %fusion.24), channel_id=1, replica_groups=mesh['sp'=8,'tp'=4] {'tp'}, dimensions={0}, use_global_device_ids=true | all-gather | bytes 983040 | tf_op jit(solution)/shard_map/all_gather | solution.py:64
  68.0 2.3 multiply_reduce_fusion.1
  70.3 8.9 %psum.23 = f32[192]{0:T(256)S(1)} all-reduce(f32[192]{0:T(256)S(1)} %get-tuple-element.45), channel_id=1, replica_groups=mesh['sp'=8,'tp'=4] {'tp'}, use_global_device_ids=true, to_apply=%region_11.12 | all-reduce | flops 192 | bytes 1536 | tf_op jit(solution)/shard_map/psum | solution.py:71
  79.8 31.1 %all_to_all.10 = bf16[32,32,512]{2,1,0:T(8,128)(2,1)} all-to-all(bf16[32,32,512]{2,1,0:T(8,128)(2,1)S(1)} %bitcast.101), channel_id=1, replica_groups=mesh['sp'=8,'tp'=4] {'sp'}, dimensions={0} | all-to-all | bytes 2097152 | tf_op jit(solution)/shard_map/all_to_all | solution.py:90
  111.1 49.4 %all-gather.2.cloned.1.call-done = bf16[32,32,2048]{2,1,0:T(8,128)(2,1)} async-done(((bf16[32,32,512]{2,1,0:T(8,128)(2,1)}), bf16[32,32,2048]{2,1,0:T(8,128)(2,1)}) %all-gather.2.cloned.1.call-update) | async-done | bytes 4194320 | tf_op jit(solution)/shard_map/all_gather | solution.py:89
  160.5 9.5 %fusion.2 = f32[4,8,32,1024]{3,2,1,0:T(8,128)S(1)} fusion(bf16[4,2048,1024]{2,1,0:T(8,128)(2,1)} %param.26, bf16[8,4,32,2048]{3,2,1,0:T(8,128)(2,1)} %bitcast.134), kind=kOutput, calls=%fused_computation.3 | convolution fusion | flops 4294967296 | bytes 25165824 | tf_op jit(solution)/shard_map/sjcd,jdf->sjcf/dot_general | solution.py:104
  170.1 12.6 %fusion.6 = bf16[8,4,32,1024]{3,2,0,1:T(8,128)(2,1)} fusion(f32[4,8,32,1024]{3,2,1,0:T(8,128)S(1)} %fusion.2, bf16[4,2048,1024]{2,1,0:T(8,128)(2,1)} %param.25, bf16[8,4,32,2048]{3,2,1,0:T(8,128)(2,1)S(1)} %bitcast.135), kind=kOutput, calls=%fused_computation.8 | convolution fusion | flops 4305453056 | bytes 27262976 | tf_op jit(solution)/shard_map/sjcd,jdf->sjcf/dot_general | solution.py:100
  182.7 12.8 %convert_bitcast_fusion = bf16[8,4,32,2048]{3,2,0,1:T(8,128)(2,1)} fusion(bf16[8,4,32,1024]{3,2,0,1:T(8,128)(2,1)} %fusion.6, bf16[4,1024,2048]{2,1,0:T(8,128)(2,1)} %param.27), kind=kOutput, calls=%fused_computation.15 | convolution fusion | flops 4297064448 | bytes 23068672 | tf_op jit(solution)/shard_map/sjcf,jfd->sjcd/dot_general | solution.py:111
  195.6 52.7 %reduce-scatter.5.cloned.1.call-done = bf16[8,4,32,512]{3,2,0,1:T(8,128)(2,1)} async-done(((bf16[8,4,32,2048]{3,2,0,1:T(8,128)(2,1)}), bf16[8,4,32,512]{3,2,0,1:T(8,128)(2,1)}) %reduce-scatter.5.cloned.1.call-update) | async-done | bytes 1048592 | tf_op jit(solution)/shard_map/reduce_scatter | solution.py:114
  248.3 2.3 copy.31
  250.6 4.6 %all-to-all-start.1 = ((bf16[32,32,512]{2,1,0:T(8,128)(2,1)}), bf16[32,32,512]{2,1,0:T(8,128)(2,1)S(1)}, u32[]{:S(2)}, u32[]{:S(2)}) async-start(bf16[32,32,512]{2,1,0:T(8,128)(2,1)} %bitcast.43), calls=%async_computation.3 | async-start | bytes 2097152 | tf_op jit(solution)/shard_map/all_to_all | solution.py:117
  256.2 25.6 %all-to-all-done.1 = bf16[32,32,512]{2,1,0:T(8,128)(2,1)S(1)} async-done(((bf16[32,32,512]{2,1,0:T(8,128)(2,1)}), bf16[32,32,512]{2,1,0:T(8,128)(2,1)S(1)}, u32[]{:S(2)}, u32[]{:S(2)}) %all-to-all-start.1) | async-done | bytes 1048608 | tf_op jit(solution)/shard_map/all_to_all | solution.py:117
  281.8 3.3 %gather_fusion = bf16[768,512]{1,0:T(8,128)(2,1)} fusion(bf16[1024,512]{1,0:T(8,128)(2,1)S(1)} %bitcast.100, s32[1024]{0:T(1024)S(1)} %pad_clamp_fusion), kind=kCustom, calls=%fused_computation | custom fusion | bytes 1575936 | tf_op jit(solution)/shard_map/gather | solution.py:125
  285.1 2.6 reshape.93
  287.7 2.5 multiply_reduce_fusion
  (46 shorter events, 6.2 us)
Async XLA Ops:
  6.5 19.2 %copy-start = (bf16[512,2048]{1,0:T(8,128)(2,1)S(1)}, bf16[512,2048]{1,0:T(8,128)(2,1)}, u32[]{:S(2)}) copy-start(bf16[512,2048]{1,0:T(8,128)(2,1)} %param.19) | copy-start | bytes 6291460
  6.5 21.5 %copy-start.4 = (s32[192,4]{0,1:T(4,128)S(1)}, s32[192,4]{0,1:T(4,128)}, u32[]{:S(2)}) copy-start(s32[192,4]{0,1:T(4,128)} %param.23) | copy-start | bytes 9220
  6.5 49.3 %copy-start.3 = (f32[2048]{0:T(1024)S(1)}, f32[2048]{0:T(1024)}, u32[]{:S(2)}) copy-start(f32[2048]{0:T(1024)} %param.20) | copy-start | bytes 24580
  6.5 48.2 %reduce-scatter.3.cloned.1.call-start = ((), (), s32[]{:S(2)}) async-start(), calls=%async_computation.4 | async-start | bytes 983040 | tf_op jit(solution)/shard_map/reduce_scatter | solution.py:54
  7.9 4.8 %collective-permute-start = (bf16[30,512]{1,0:T(8,128)(2,1)S(1)}, bf16[30,512]{1,0:T(8,128)(2,1)S(1)}, u32[]{:S(2)}, u32[]{:S(2)}) collective-permute-start(bf16[30,512]{1,0:T(8,128)(2,1)S(1)} %slice.258), channel_id=1, source_target_pairs={{0,4},{4,8},{8,12},{12,16},{16,20},{20,24},{24,28},{1,5},{5,9},{9,... | collective-permute-start | bytes 92168 | tf_op jit(solution)/shard_map/ppermute | solution.py:17
  14.9 53.2 %copy-start.2 = (bf16[192,512]{1,0:T(8,128)(2,1)S(1)}, bf16[192,512]{1,0:T(8,128)(2,1)}, u32[]{:S(2)}) copy-start(bf16[192,512]{1,0:T(8,128)(2,1)} %param.14) | copy-start | bytes 589828
  28.0 51.2 %copy-start.6 = (f32[512]{0:T(512)S(1)}, f32[512]{0:T(512)}, u32[]{:S(2)}) copy-start(f32[512]{0:T(512)} %param.22) | copy-start | bytes 6148
  28.0 132.5 %all-gather.2.cloned.1.call-start = ((), (), s32[]{:S(2)}) async-start(), calls=%async_computation.5 | async-start | bytes 5242880 | tf_op jit(solution)/shard_map/all_gather | solution.py:89
  110.9 137.4 %reduce-scatter.5.cloned.1.call-start = ((), (), s32[]{:S(2)}) async-start(), calls=%async_computation.6 | async-start | bytes 5242880 | tf_op jit(solution)/shard_map/reduce_scatter | solution.py:114
  160.5 9.5 %copy-start.7 = (bf16[32,32,2048]{2,1,0:T(8,128)(2,1)S(1)}, bf16[32,32,2048]{2,1,0:T(8,128)(2,1)}, u32[]{:S(2)}) copy-start(bf16[32,32,2048]{2,1,0:T(8,128)(2,1)} %all-gather.2.cloned.1.call-done) | copy-start | bytes 12582916
  195.6 59.8 %copy-start.5 = (f32[192,4]{0,1:T(4,128)S(1)}, f32[192,4]{0,1:T(4,128)}, u32[]{:S(2)}) copy-start(f32[192,4]{0,1:T(4,128)} %param.24) | copy-start | bytes 9220
  250.6 31.2 %all-to-all-start.1 = ((bf16[32,32,512]{2,1,0:T(8,128)(2,1)}), bf16[32,32,512]{2,1,0:T(8,128)(2,1)S(1)}, u32[]{:S(2)}, u32[]{:S(2)}) async-start(bf16[32,32,512]{2,1,0:T(8,128)(2,1)} %bitcast.43), calls=%async_computation.3 | async-start | bytes 2097152 | tf_op jit(solution)/shard_map/all_to_all | solution.py:117
  281.8 9.1 %copy-start.1 = (bf16[512,2048]{1,0:T(8,128)(2,1)S(1)}, bf16[512,2048]{1,0:T(8,128)(2,1)}, u32[]{:S(2)}) copy-start(bf16[512,2048]{1,0:T(8,128)(2,1)} %param.19) | copy-start | bytes 6291460
Sparse Core Ops, SparseCore 0:
  28.2 26.5 reduce-scatter.2
  111.0 49.4 all-gather.1
  195.7 52.5 reduce-scatter.4
where the time goes:
time: 298 us; the launch traced here: 297 us
  waiting for transfers between devices  151 us (51%)
  blocking collectives  62 us (21%)
  matrix products  40.1 us (13%)
  between operations  13.3 us (4%)
  local copies, waits for them, and re-layouts  12.3 us (4%)
  other arithmetic  11.3 us (4%)
  starting transfers between devices  7.27 us (2%)
    reduce_scatter x1, waiting for transfers between devices, shards(): lax.psum_scatter(partial_value.astype(jnp.bfloat16), 'tp', scatter_dimens...  52.7 us
    all_gather x1, waiting for transfers between devices, shards(): lax.all_gather(lax.all_to_all(outgoing, 'sp', split_axis=0, concat_axis=0...  49.4 us
    all_to_all x1, blocking collectives, shards(): lax.all_to_all(outgoing, 'sp', split_axis=0, concat_axis=0, tiled=True)  31.1 us
    all_to_all x1, waiting for transfers between devices, shards(): lax.all_to_all(summed.reshape(sources * local_experts, count, summed.shap...  25.6 us
    reduce_scatter x1, waiting for transfers between devices, shards(): lax.psum_scatter(jnp.dot(act, point_weight, preferred_element_type=jnp.fl...  23.3 us
    dot_general x1, matrix products, shards(): jnp.einsum('sjcf,jfd->sjcd', hidden, down_experts, preferred_element_type...  12.8 us
    dot_general x1, matrix products, shards(): jnp.einsum('sjcd,jdf->sjcf', rows, gate_experts, preferred_element_type=j...  12.6 us
    all_gather x1, blocking collectives, shards(): lax.all_gather(mixed, 'tp', axis=0, tiled=True)  11.2 us
  transfers between devices with their start and end apart: 5, of which 4 were waited for; matrix products, arithmetic and copies ran while one was open for 2% of the time, Pallas kernels for 0%

commit v1 on v0

--- a/solution.py
+++ b/solution.py
@@ -9,6 +9,10 @@
 epsilon = 1e-05
 clamp_limit = 7.0
 swish_slope = 1.702
+
+
+def touch_plate_by_axis(patch, along_axis):
+    return jnp.concatenate(lax.all_gather(patch, along_axis), axis=2)
 
 
 def from_behind(block, axis, distance):
@@ -86,11 +90,8 @@
         .astype(jnp.bfloat16)
         .reshape(E, CAP, feat_local)
     )
-    received = lax.all_gather(
-        lax.all_to_all(outgoing, "sp", split_axis=0, concat_axis=0, tiled=True),
-        "tp",
-        axis=2,
-        tiled=True,
+    received = touch_plate_by_axis(
+        lax.all_to_all(outgoing, "sp", split_axis=0, concat_axis=0, tiled=True), "tp"
     )
     local_experts = gate_experts.shape[0]
     sources = received.shape[0] // local_experts

time: 298 us -> 312 us (1.047)
  local copies, waits for them, and re-layouts: 12.3 us -> 28.2 us
    reshape x0 -> x1, local copies, waits for them, and re-layouts: none -> 8.12 us  [touch_plate_by_axis(): return jnp.concatenate(lax.all_gather(patch, along_axis), axis=2)]
    another operation x0 -> x1, local copies, waits for them, and re-layouts: none -> 7.75 us  [shards(): rows = received.reshape(sources, local_experts, count, received.shape[2])]
where the time goes in v1:
time: 312 us; the launch traced here: 311 us
  waiting for transfers between devices  152 us (49%)
  blocking collectives  62 us (20%)
  matrix products  37.8 us (12%)
  local copies, waits for them, and re-layouts  28.2 us (9%)
  between operations  13.3 us (4%)
  other arithmetic  11.3 us (4%)
  starting transfers between devices  7.09 us (2%)
    reduce_scatter x1, waiting for transfers between devices, shards(): lax.psum_scatter(partial_value.astype(jnp.bfloat16), 'tp', scatter_dimens...  52.8 us
    all_gather x1, waiting for transfers between devices, touch_plate_by_axis(): return jnp.concatenate(lax.all_gather(patch, along_axis), axis=2)  49.7 us
    all_to_all x1, blocking collectives, shards(): lax.all_to_all(outgoing, 'sp', split_axis=0, concat_axis=0, tiled=True)  31.1 us
    all_to_all x1, waiting for transfers between devices, shards(): lax.all_to_all(summed.reshape(sources * local_experts, count, summed.shap...  25.6 us
    reduce_scatter x1, waiting for transfers between devices, shards(): lax.psum_scatter(jnp.dot(act, point_weight, preferred_element_type=jnp.fl...  23.3 us
    dot_general x1, matrix products, shards(): jnp.einsum('sjcf,jfd->sjcd', hidden, down_experts, preferred_element_type...  11.9 us
    dot_general x1, matrix products, shards(): jnp.einsum('sjcd,jdf->sjcf', rows, gate_experts, preferred_element_type=j...  11.3 us
    all_gather x1, blocking collectives, shards(): lax.all_gather(mixed, 'tp', axis=0, tiled=True)  11.2 us
  transfers between devices with their start and end apart: 5, of which 4 were waited for; matrix products, arithmetic and copies ran while one was open for 2% of the time, Pallas kernels for 0%

profile of v1, /device:TPU:0, one launch (start us, length us, event | category | flops | bytes accessed | tf_op | source)
XLA Modules:
  0.0 311.2 jit_solution(3439611317738213485)
XLA Ops:
  6.5 1.3 multiply_convert_fusion.2
  7.9 2.4 collective-permute-start
  12.6 2.2 fusion.67
  14.9 10.9 %all-reduce = (f32[192]{0:T(256)S(1)}, f32[192]{0:T(256)S(1)}) all-reduce(f32[192]{0:T(256)S(1)} %get-tuple-element.6, f32[192]{0:T(256)S(1)} %get-tuple-element.5), channel_id=1, replica_groups=mesh['sp'=8,'tp'=4] {'tp'}, use_global_device_ids=true, to_apply=%region_3.0 | all-reduce | flops 384 | bytes 3072 | tf_op jit(solution)/shard_map/psum | solution.py:52
  25.8 2.2 convolution_convert_fusion
  28.5 1.7 reduce-window.6
  31.4 23.3 %reduce-scatter.3.cloned.1.call-done = bf16[48,2048]{1,0:T(8,128)(2,1)} async-done(((bf16[192,2048]{1,0:T(8,128)(2,1)}), bf16[48,2048]{1,0:T(8,128)(2,1)}) %reduce-scatter.3.cloned.1.call-update) | async-done | bytes 196624 | tf_op jit(solution)/shard_map/reduce_scatter | solution.py:58
  56.8 11.2 %all_gather.9 = bf16[192,2048]{1,0:T(8,128)(2,1)S(1)} all-gather(bf16[48,2048]{1,0:T(8,128)(2,1)S(1)} %fusion.24), channel_id=1, replica_groups=mesh['sp'=8,'tp'=4] {'tp'}, dimensions={0}, use_global_device_ids=true | all-gather | bytes 983040 | tf_op jit(solution)/shard_map/all_gather | solution.py:68
  68.0 2.3 multiply_reduce_fusion.1
  70.3 8.9 %psum.23 = f32[192]{0:T(256)S(1)} all-reduce(f32[192]{0:T(256)S(1)} %get-tuple-element.45), channel_id=1, replica_groups=mesh['sp'=8,'tp'=4] {'tp'}, use_global_device_ids=true, to_apply=%region_11.12 | all-reduce | flops 192 | bytes 1536 | tf_op jit(solution)/shard_map/psum | solution.py:75
  79.8 31.1 %all_to_all.10 = bf16[32,32,512]{2,1,0:T(8,128)(2,1)} all-to-all(bf16[32,32,512]{2,1,0:T(8,128)(2,1)S(1)} %bitcast.104), channel_id=1, replica_groups=mesh['sp'=8,'tp'=4] {'sp'}, dimensions={0} | all-to-all | bytes 2097152 | tf_op jit(solution)/shard_map/all_to_all | solution.py:94
  110.9 49.7 %all-gather.3.cloned.1.call-done = bf16[128,32,512]{2,1,0:T(8,128)(2,1)} async-done(((bf16[32,32,512]{2,1,0:T(8,128)(2,1)}), bf16[128,32,512]{2,1,0:T(8,128)(2,1)}) %all-gather.3.cloned.1.call-update) | async-done | bytes 4194320 | tf_op jit(solution)/shard_map/all_gather | solution.py:15
  160.7 8.1 %copy.47 = bf16[32,32,4,512]{3,2,1,0:T(4,128)(2,1)} copy(bf16[32,32,4,512]{3,1,0,2:T(8,128)(2,1)} %bitcast.103) | data formatting | bytes 8388608 | tf_op jit(solution)/shard_map/reshape | solution.py:15
  168.8 7.7 %reshape_reshape.3 = bf16[8,4,32,2048]{3,2,1,0:T(8,128)(2,1)} reshape(bf16[32,32,4,512]{3,2,1,0:T(4,128)(2,1)} %copy.47) | data formatting | bytes 8388608 | tf_op jit(solution)/shard_map/reshape;reshape | solution.py:99
  176.5 9.5 %fusion.2 = f32[4,8,32,1024]{3,2,1,0:T(8,128)S(1)} fusion(bf16[4,2048,1024]{2,1,0:T(8,128)(2,1)} %param.26, bf16[8,4,32,2048]{3,2,1,0:T(8,128)(2,1)} %reshape_reshape.3), kind=kOutput, calls=%fused_computation.3 | convolution fusion | flops 4294967296 | bytes 25165824 | tf_op jit(solution)/shard_map/sjcd,jdf->sjcf/dot_general | solution.py:105
  186.1 11.3 %fusion.6 = bf16[8,4,32,1024]{3,2,0,1:T(8,128)(2,1)S(1)} fusion(f32[4,8,32,1024]{3,2,1,0:T(8,128)S(1)} %fusion.2, bf16[4,2048,1024]{2,1,0:T(8,128)(2,1)} %param.25, bf16[8,4,32,2048]{3,2,1,0:T(8,128)(2,1)S(1)} %copy-done.2), kind=kOutput, calls=%fused_computation.8 | convolution fusion | flops 4305453056 | bytes 27262976 | tf_op jit(solution)/shard_map/sjcd,jdf->sjcf/dot_general | solution.py:101
  197.4 11.9 %convert_bitcast_fusion = bf16[8,4,32,2048]{3,2,0,1:T(8,128)(2,1)} fusion(bf16[8,4,32,1024]{3,2,0,1:T(8,128)(2,1)S(1)} %fusion.6, bf16[4,1024,2048]{2,1,0:T(8,128)(2,1)} %param.27), kind=kOutput, calls=%fused_computation.15 | convolution fusion | flops 4297064448 | bytes 23068672 | tf_op jit(solution)/shard_map/sjcf,jfd->sjcd/dot_general | solution.py:112
  209.3 52.8 %reduce-scatter.5.cloned.1.call-done = bf16[8,4,32,512]{3,2,0,1:T(8,128)(2,1)} async-done(((bf16[8,4,32,2048]{3,2,0,1:T(8,128)(2,1)}), bf16[8,4,32,512]{3,2,0,1:T(8,128)(2,1)}) %reduce-scatter.5.cloned.1.call-update) | async-done | bytes 1048592 | tf_op jit(solution)/shard_map/reduce_scatter | solution.py:115
  262.1 2.3 copy.50
  264.4 4.6 %all-to-all-start.1 = ((bf16[32,32,512]{2,1,0:T(8,128)(2,1)}), bf16[32,32,512]{2,1,0:T(8,128)(2,1)S(1)}, u32[]{:S(2)}, u32[]{:S(2)}) async-start(bf16[32,32,512]{2,1,0:T(8,128)(2,1)} %bitcast.44), calls=%async_computation.3 | async-start | bytes 2097152 | tf_op jit(solution)/shard_map/all_to_all | solution.py:118
  269.9 25.6 %all-to-all-done.1 = bf16[32,32,512]{2,1,0:T(8,128)(2,1)S(1)} async-done(((bf16[32,32,512]{2,1,0:T(8,128)(2,1)}), bf16[32,32,512]{2,1,0:T(8,128)(2,1)S(1)}, u32[]{:S(2)}, u32[]{:S(2)}) %all-to-all-start.1) | async-done | bytes 1048608 | tf_op jit(solution)/shard_map/all_to_all | solution.py:118
  295.6 3.3 %gather_fusion = bf16[768,512]{1,0:T(8,128)(2,1)} fusion(bf16[1024,512]{1,0:T(8,128)(2,1)S(1)} %bitcast.102, s32[1024]{0:T(1024)S(1)} %pad_clamp_fusion), kind=kCustom, calls=%fused_computation | custom fusion | bytes 1575936 | tf_op jit(solution)/shard_map/gather | solution.py:126
  298.9 2.6 reshape.93
  301.5 2.5 multiply_reduce_fusion
  (48 shorter events, 8.4 us)
Async XLA Ops:
  6.5 19.2 %copy-start = (bf16[512,2048]{1,0:T(8,128)(2,1)S(1)}, bf16[512,2048]{1,0:T(8,128)(2,1)}, u32[]{:S(2)}) copy-start(bf16[512,2048]{1,0:T(8,128)(2,1)} %param.19) | copy-start | bytes 6291460
  6.5 21.5 %copy-start.5 = (s32[192,4]{0,1:T(4,128)S(1)}, s32[192,4]{0,1:T(4,128)}, u32[]{:S(2)}) copy-start(s32[192,4]{0,1:T(4,128)} %param.23) | copy-start | bytes 9220
  6.5 49.3 %copy-start.4 = (f32[2048]{0:T(1024)S(1)}, f32[2048]{0:T(1024)}, u32[]{:S(2)}) copy-start(f32[2048]{0:T(1024)} %param.20) | copy-start | bytes 24580
  6.5 48.2 %reduce-scatter.3.cloned.1.call-start = ((), (), s32[]{:S(2)}) async-start(), calls=%async_computation.4 | async-start | bytes 983040 | tf_op jit(solution)/shard_map/reduce_scatter | solution.py:58
  7.9 4.8 %collective-permute-start = (bf16[30,512]{1,0:T(8,128)(2,1)S(1)}, bf16[30,512]{1,0:T(8,128)(2,1)S(1)}, u32[]{:S(2)}, u32[]{:S(2)}) collective-permute-start(bf16[30,512]{1,0:T(8,128)(2,1)S(1)} %slice.258), channel_id=1, source_target_pairs={{0,4},{4,8},{8,12},{12,16},{16,20},{20,24},{24,28},{1,5},{5,9},{9,... | collective-permute-start | bytes 92168 | tf_op jit(solution)/shard_map/ppermute | solution.py:21
  14.9 53.2 %copy-start.3 = (bf16[192,512]{1,0:T(8,128)(2,1)S(1)}, bf16[192,512]{1,0:T(8,128)(2,1)}, u32[]{:S(2)}) copy-start(bf16[192,512]{1,0:T(8,128)(2,1)} %param.14) | copy-start | bytes 589828
  28.0 51.2 %copy-start.7 = (f32[512]{0:T(512)S(1)}, f32[512]{0:T(512)}, u32[]{:S(2)}) copy-start(f32[512]{0:T(512)} %param.22) | copy-start | bytes 6148
  28.0 132.6 %all-gather.3.cloned.1.call-start = ((), (), s32[]{:S(2)}) async-start(), calls=%async_computation.6 | async-start | bytes 5242880 | tf_op jit(solution)/shard_map/all_gather | solution.py:15
  110.9 151.2 %reduce-scatter.5.cloned.1.call-start = ((), (), s32[]{:S(2)}) async-start(), calls=%async_computation.5 | async-start | bytes 5242880 | tf_op jit(solution)/shard_map/reduce_scatter | solution.py:115
  176.5 9.5 %copy-start.2 = (bf16[8,4,32,2048]{3,2,1,0:T(8,128)(2,1)S(1)}, bf16[8,4,32,2048]{3,2,1,0:T(8,128)(2,1)}, u32[]{:S(2)}) copy-start(bf16[8,4,32,2048]{3,2,1,0:T(8,128)(2,1)} %reshape_reshape.3) | copy-start | bytes 12582916
  209.3 59.8 %copy-start.6 = (f32[192,4]{0,1:T(4,128)S(1)}, f32[192,4]{0,1:T(4,128)}, u32[]{:S(2)}) copy-start(f32[192,4]{0,1:T(4,128)} %param.24) | copy-start | bytes 9220
  264.4 31.2 %all-to-all-start.1 = ((bf16[32,32,512]{2,1,0:T(8,128)(2,1)}), bf16[32,32,512]{2,1,0:T(8,128)(2,1)S(1)}, u32[]{:S(2)}, u32[]{:S(2)}) async-start(bf16[32,32,512]{2,1,0:T(8,128)(2,1)} %bitcast.44), calls=%async_computation.3 | async-start | bytes 2097152 | tf_op jit(solution)/shard_map/all_to_all | solution.py:118
  295.6 9.1 %copy-start.1 = (bf16[512,2048]{1,0:T(8,128)(2,1)S(1)}, bf16[512,2048]{1,0:T(8,128)(2,1)}, u32[]{:S(2)}) copy-start(bf16[512,2048]{1,0:T(8,128)(2,1)} %param.19) | copy-start | bytes 6291460
Sparse Core Ops, SparseCore 0:
  28.2 26.5 reduce-scatter.2
  111.0 49.6 all-gather.2
  209.4 52.5 reduce-scatter.4
